TPU v7x, 32 devices: a whole 2x2x4 slice. The times are simulated.
32 devices in a mesh: sp: 8 (over z, y), tp: 4 (over x, core).
Axes of the slice: x: 2, y: 2, z: 4, core: 2. Of those that a mesh axis runs over, the one named last changes fastest.
Arguments:
- queries: bfloat16 [4096, 2048], P('sp', 'tp'), may hold values from -8 to 8
- keys: bfloat16 [4096, 512], P('sp', 'tp'), may hold values from -8 to 8
- values: bfloat16 [4096, 512], P('sp', 'tp'), may hold values from -6 to 6
- q_gain: float32 [128], replicated, may hold values from 0.1 to 5.8
- k_gain: float32 [128], replicated, may hold values from 0.1 to 5.8
- out_weight: bfloat16 [2048, 2048], replicated, may hold values from -0.125 to 0.125
- out_gain: float32 [2048], replicated, may hold values from 0.1 to 1.9
- residual_in: bfloat16 [4096, 2048], P(('sp', 'tp')), may hold values from -6 to 6
- mlp_gain: float32 [2048], replicated, may hold values from 0.1 to 1.9
- gate_weight: bfloat16 [2048, 5632], P('sp', 'tp'), may hold values from -0.125 to 0.125
- up_weight: bfloat16 [2048, 5632], P('sp', 'tp'), may hold values from -0.125 to 0.125
- down_weight: bfloat16 [5632, 2048], P('tp', 'sp'), may hold values from -0.078125 to 0.078125
- final_gain: float32 [2048], replicated, may hold values from 0.1 to 1.9
Outputs:
- layer_out: bfloat16 [4096, 2048], P(('sp', 'tp'))
All inputs are finite; a program needn't handle non-finite values.
Results may differ from a plain program's by a relative error of at most 0.015.
The roundings to bfloat16 on the way count: a program that leaves them out, or rounds other values in their place, can miss the bound.
Values may be sent and summed in bfloat16 or wider, within the bound.
A program may use at most 128 MiB of HBM per device.

v0:
```python
import math
import jax
import jax.numpy as jnp
from jax import lax
from jax.sharding import PartitionSpec as P

GRID_W = 64


def rms_scale(matrix):
    return matrix * lax.rsqrt(jnp.mean(matrix * matrix, axis=-1, keepdims=True) + 1e-06)


def rotary(matrix, positions):
    quarter = matrix.shape[-1] // 4
    freqs = 10000.0 ** (-jnp.arange(quarter, dtype=jnp.float32) / quarter)
    grid = jnp.stack([positions // GRID_W, positions % GRID_W], axis=-1).astype(jnp.float32)
    angle = grid[:, :, None] * freqs
    cosine = jnp.cos(angle)[:, None]
    sine = jnp.sin(angle)[:, None]
    parts = matrix.reshape(matrix.shape[:-1] + (2, 2, quarter))
    first = parts[..., 0, :]
    second = parts[..., 1, :]
    turned = jnp.stack([first * cosine - second * sine, second * cosine + first * sine], axis=-2)
    return turned.reshape(matrix.shape)


def on_device(
    queries,
    keys,
    values,
    q_gain,
    k_gain,
    out_weight,
    out_gain,
    residual_in,
    mlp_gain,
    gate_weight,
    up_weight,
    down_weight,
    final_gain,
):
    tok_rows = queries.shape[0]
    head_size = q_gain.shape[0]
    q_heads = queries.shape[1] // head_size
    kv_heads = keys.shape[1] // head_size
    group_size = q_heads // kv_heads
    positions = lax.axis_index("sp") * tok_rows + jnp.arange(tok_rows, dtype=jnp.int32)
    query_rot = rotary(
        rms_scale(queries.reshape(tok_rows, q_heads, head_size).astype(jnp.float32)) * q_gain,
        positions,
    ).astype(jnp.bfloat16)
    key_rot = rotary(
        rms_scale(keys.reshape(tok_rows, kv_heads, head_size).astype(jnp.float32)) * k_gain,
        positions,
    ).astype(jnp.bfloat16)
    key_flat = key_rot.reshape(tok_rows, kv_heads * head_size)
    grouped = query_rot.reshape(tok_rows, kv_heads, group_size, head_size)
    score_scale = head_size ** (-0.5)
    key_all, value_all = (
        lax.all_gather(key_flat, "sp", axis=0, tiled=True),
        lax.all_gather(values, "sp", axis=0, tiled=True),
    )
    total_rows = key_all.shape[0]
    span = math.gcd(total_rows, 1024)
    key_blocks = key_all.reshape(total_rows // span, span, kv_heads, head_size)
    value_blocks = value_all.reshape(total_rows // span, span, kv_heads, head_size)

    def step(run_state, blocks):
        highest, weight_sum, accum = run_state
        key_block, value_block = blocks
        scores = (
            jnp.einsum("qcgd,kcd->cgqk", grouped, key_block, preferred_element_type=jnp.float32)
            * score_scale
        )
        new_high = jnp.maximum(highest, jnp.max(scores, axis=-1))
        factor = jnp.exp(highest - new_high)
        exp_scores = jnp.exp(scores - new_high[..., None])
        weight_sum = weight_sum * factor + jnp.sum(exp_scores, axis=-1)
        accum = accum * factor[..., None] + jnp.einsum(
            "cgqk,kcd->cgqd",
            exp_scores.astype(jnp.bfloat16),
            value_block,
            preferred_element_type=jnp.float32,
        )
        return ((new_high, weight_sum, accum), None)

    start_state = (
        jnp.full((kv_heads, group_size, tok_rows), -1e30, jnp.float32),
        jnp.zeros((kv_heads, group_size, tok_rows), jnp.float32),
        jnp.zeros((kv_heads, group_size, tok_rows, head_size), jnp.float32),
    )
    final_state, unused = lax.scan(step, start_state, (key_blocks, value_blocks))
    highest, weight_sum, accum = final_state
    attended = (
        jnp.transpose(accum / weight_sum[..., None], (2, 0, 1, 3))
        .reshape(tok_rows, q_heads * head_size)
        .astype(jnp.bfloat16)
    )
    head_rows = lax.all_to_all(attended, "tp", split_axis=0, concat_axis=1, tiled=True)
    projected = jnp.dot(head_rows, out_weight, preferred_element_type=jnp.float32)
    mid_stream = (residual_in.astype(jnp.float32) + out_gain * rms_scale(projected)).astype(
        jnp.bfloat16
    )
    normed = (mlp_gain * rms_scale(mid_stream.astype(jnp.float32))).astype(jnp.bfloat16)
    mixer_in = lax.all_gather(normed, "tp", axis=0, tiled=True)
    gate_proj = jnp.dot(
        mixer_in,
        lax.all_gather(gate_weight, "sp", axis=0, tiled=True),
        preferred_element_type=jnp.float32,
    )
    up_proj = jnp.dot(
        mixer_in,
        lax.all_gather(up_weight, "sp", axis=0, tiled=True),
        preferred_element_type=jnp.float32,
    )
    down_full = lax.all_gather(down_weight, "sp", axis=1, tiled=True)
    hidden = (jax.nn.silu(gate_proj) * up_proj).astype(jnp.bfloat16)
    mlp_branch = lax.psum_scatter(
        jnp.dot(hidden, down_full, preferred_element_type=jnp.float32).astype(jnp.bfloat16),
        "tp",
        scatter_dimension=0,
        tiled=True,
    ).astype(jnp.float32)
    return (mid_stream.astype(jnp.float32) + final_gain * rms_scale(mlp_branch)).astype(
        jnp.bfloat16
    )


def solution(mesh):
    return jax.shard_map(
        on_device,
        mesh=mesh,
        in_specs=(
            P("sp", "tp"),
            P("sp", "tp"),
            P("sp", "tp"),
            P(),
            P(),
            P(),
            P(),
            P(("sp", "tp"), None),
            P(),
            P("sp", "tp"),
            P("sp", "tp"),
            P("tp", "sp"),
            P(),
        ),
        out_specs=P(("sp", "tp"), None),
        check_vma=False,
    )
```

profile of v0, /device:TPU:0, one launch (start us, length us, event | category | flops | bytes accessed | tf_op | source)
XLA Modules:
  0.0 513.3 jit_solution(11249257965567632647)
XLA Ops:
  13.9 38.1 %all-gather.7.cloned.1.call-done = bf16[4096,128]{0,1:T(8,128)(2,1)} async-done(((bf16[512,128]{0,1:T(8,128)(2,1)}), bf16[4096,128]{0,1:T(8,128)(2,1)}) %all-gather.7.cloned.1.call-update) | async-done | bytes 1048592 | tf_op jit(solution)/shard_map/all_gather | solution.py:61
  52.0 1.6 copy.24
  53.6 39.8 %all-gather.9.cloned.1.call-done = bf16[4096,128]{1,0:T(8,128)(2,1)} async-done(((bf16[512,128]{1,0:T(8,128)(2,1)}), bf16[4096,128]{1,0:T(8,128)(2,1)}) %all-gather.9.cloned.1.call-update) | async-done | bytes 1048592 | tf_op jit(solution)/shard_map/all_gather | solution.py:62
  93.4 47.3 %while.15 = (s32[]{:T(128)}, f32[1,4,512]{2,1,0:T(4,128)S(1)}, f32[1,4,512]{2,1,0:T(4,128)S(1)}, f32[1,4,512,128]{3,2,1,0:T(8,128)S(1)}, bf16[4,1024,1,128]{3,1,...) while((s32[]{:T(128)}, f32[1,4,512]{2,1,0:T(4,128)S(1)}, ...), condition=%wide.region_5.6_spmd.clone, body=%wide.region_2.5_spmd.clone.sunk | while | flops 1091317760 | bytes 61997704 | solution.py:93
  93.4 4.5 bitcast_reduce_fusion.3
  97.9 4.6 fusion.60
  105.2 4.5 bitcast_reduce_fusion.3
  109.7 4.6 fusion.60
  117.0 4.5 bitcast_reduce_fusion.3
  121.5 4.6 fusion.60
  127.4 1.4 fusion.59
  128.9 4.5 bitcast_reduce_fusion.3
  133.4 4.6 fusion.60
  139.3 1.4 fusion.59
  141.7 11.4 %all_to_all.16 = bf16[4,128,512]{2,1,0:T(8,128)(2,1)S(1)} all-to-all(bf16[4,128,512]{2,1,0:T(8,128)(2,1)S(1)} %convert_element_type.88), channel_id=1, replica_groups=mesh['sp'=8,'tp'=4] {'tp'}, dimensions={0} | all-to-all | bytes 1048576 | tf_op jit(solution)/shard_map/all_to_all | solution.py:100
  153.3 4.8 multiply_reduce_fusion
  161.5 18.5 %all-gather.11.cloned.1.call-done = bf16[512,2048]{1,0:T(8,128)(2,1)} async-done(((bf16[128,2048]{1,0:T(8,128)(2,1)}), bf16[512,2048]{1,0:T(8,128)(2,1)}) %all-gather.11.cloned.1.call-update) | async-done | bytes 2097168 | tf_op jit(solution)/shard_map/all_gather | solution.py:106
  180.1 94.4 %all-gather.13.cloned.1.call-done = bf16[2048,1408]{1,0:T(8,128)(2,1)} async-done(((bf16[256,1408]{1,0:T(8,128)(2,1)}), bf16[2048,1408]{1,0:T(8,128)(2,1)}) %all-gather.13.cloned.1.call-update) | async-done | bytes 5767184 | tf_op jit(solution)/shard_map/all_gather | solution.py:109
  274.4 8.2 %fusion.43 = f32[512,1408]{1,0:T(8,128)} fusion(bf16[512,2048]{1,0:T(8,128)(2,1)} %all-gather.11.cloned.1.call-done, bf16[2048,1408]{1,0:T(8,128)(2,1)} %all-gather.13.cloned.1.call-done), kind=kOutput, calls=%fused_computation.81 | convolution fusion | flops 2952790016 | bytes 10747904 | tf_op jit(solution)/shard_map/dot_general | solution.py:107
  282.7 84.3 %all-gather.15.cloned.1.call-done = bf16[2048,1408]{1,0:T(8,128)(2,1)} async-done(((bf16[256,1408]{1,0:T(8,128)(2,1)}), bf16[2048,1408]{1,0:T(8,128)(2,1)}) %all-gather.15.cloned.1.call-update) | async-done | bytes 5767184 | tf_op jit(solution)/shard_map/all_gather | solution.py:114
  367.0 93.2 %all-gather.17.cloned.1.call-done = bf16[1408,2048]{1,0:T(8,128)(2,1)} async-done(((bf16[1408,256]{1,0:T(8,128)(2,1)}), bf16[1408,2048]{1,0:T(8,128)(2,1)}) %all-gather.17.cloned.1.call-update) | async-done | bytes 5767184 | tf_op jit(solution)/shard_map/all_gather | solution.py:117
  460.2 13.3 %convolution_convert_fusion = bf16[512,2048]{1,0:T(8,128)(2,1)} fusion(bf16[1408,2048]{1,0:T(8,128)(2,1)} %all-gather.17.cloned.1.call-done, bf16[512,2048]{1,0:T(8,128)(2,1)S(1)} %copy-done.5, bf16[2048,1408]{1,0:T(8,128)(2,1)} %all-gather.15.cloned.1.call-done, f32[512,1408]{1,0:T(8,128)} %fusion.43), kind=kOutput, calls=%fused_computation.28 | convolution fusion | flops 5910953984 | bytes 18612224 | tf_op jit(solution)/shard_map/dot_general | solution.py:120
  473.6 29.5 %reduce-scatter.2.cloned.1.call-done = bf16[128,2048]{1,0:T(8,128)(2,1)} async-done(((bf16[512,2048]{1,0:T(8,128)(2,1)}), bf16[128,2048]{1,0:T(8,128)(2,1)}) %reduce-scatter.2.cloned.1.call-update) | async-done | bytes 524304 | tf_op jit(solution)/shard_map/reduce_scatter | solution.py:119
  504.3 2.1 fusion.30
  (77 shorter events, 21.1 us)
Async XLA Ops:
  6.5 45.4 %all-gather.7.cloned.1.call-start = ((), (), s32[]{:S(2)}) async-start(), calls=%async_computation.2 | async-start | bytes 1179648 | tf_op jit(solution)/shard_map/all_gather | solution.py:61
  9.7 83.7 %all-gather.9.cloned.1.call-start = ((), (), s32[]{:S(2)}) async-start(), calls=%async_computation.3 | async-start | bytes 1179648 | tf_op jit(solution)/shard_map/all_gather | solution.py:62
  10.4 169.6 %all-gather.11.cloned.1.call-start = ((), (), s32[]{:S(2)}) async-start(), calls=%async_computation.4 | async-start | bytes 2621440 | tf_op jit(solution)/shard_map/all_gather | solution.py:106
  97.9 5.9 %copy-start = (f32[1024,512,4]{1,0,2:T(8,128)S(1)}, f32[1024,512,4]{1,0,2:T(8,128)}, u32[]{:S(2)}) copy-start(f32[1024,512,4]{1,0,2:T(8,128)} %get-tuple-element.155) | copy-start | bytes 25165828 | tf_op jit(solution)/shard_map/while
  109.7 5.9 %copy-start = (f32[1024,512,4]{1,0,2:T(8,128)S(1)}, f32[1024,512,4]{1,0,2:T(8,128)}, u32[]{:S(2)}) copy-start(f32[1024,512,4]{1,0,2:T(8,128)} %get-tuple-element.155) | copy-start | bytes 25165828 | tf_op jit(solution)/shard_map/while
  121.5 5.9 %copy-start = (f32[1024,512,4]{1,0,2:T(8,128)S(1)}, f32[1024,512,4]{1,0,2:T(8,128)}, u32[]{:S(2)}) copy-start(f32[1024,512,4]{1,0,2:T(8,128)} %get-tuple-element.155) | copy-start | bytes 25165828 | tf_op jit(solution)/shard_map/while
  133.3 5.9 %copy-start = (f32[1024,512,4]{1,0,2:T(8,128)S(1)}, f32[1024,512,4]{1,0,2:T(8,128)}, u32[]{:S(2)}) copy-start(f32[1024,512,4]{1,0,2:T(8,128)} %get-tuple-element.155) | copy-start | bytes 25165828 | tf_op jit(solution)/shard_map/while
  153.3 4.8 copy-start.1
  153.3 4.8 copy-start.2
  153.3 5.2 %copy-start.3 = (f32[2048]{0:T(1024)S(1)}, f32[2048]{0:T(1024)}, u32[]{:S(2)}) copy-start(f32[2048]{0:T(1024)} %param.23) | copy-start | bytes 24580
  159.5 114.9 %all-gather.13.cloned.1.call-start = ((), (), s32[]{:S(2)}) async-start(), calls=%async_computation.5 | async-start | bytes 6488064 | tf_op jit(solution)/shard_map/all_gather | solution.py:109
  160.1 206.9 %all-gather.15.cloned.1.call-start = ((), (), s32[]{:S(2)}) async-start(), calls=%async_computation.6 | async-start | bytes 6488064 | tf_op jit(solution)/shard_map/all_gather | solution.py:114
  160.7 299.5 %all-gather.17.cloned.1.call-start = ((), (), s32[]{:S(2)}) async-start(), calls=%async_computation.7 | async-start | bytes 6488064 | tf_op jit(solution)/shard_map/all_gather | solution.py:117
  161.3 341.8 %reduce-scatter.2.cloned.1.call-start = ((), (), s32[]{:S(2)}) async-start(), calls=%async_computation.8 | async-start | bytes 2621440 | tf_op jit(solution)/shard_map/reduce_scatter | solution.py:119
  180.1 280.2 %copy-start.5 = (bf16[512,2048]{1,0:T(8,128)(2,1)S(1)}, bf16[512,2048]{1,0:T(8,128)(2,1)}, u32[]{:S(2)}) copy-start(bf16[512,2048]{1,0:T(8,128)(2,1)} %all-gather.11.cloned.1.call-done) | copy-start | bytes 6291460
  282.7 221.7 %copy-start.4 = (f32[2048]{0:T(1024)S(1)}, f32[2048]{0:T(1024)}, u32[]{:S(2)}) copy-start(f32[2048]{0:T(1024)} %param.27) | copy-start | bytes 24580
Sparse Core Ops, SparseCore 0:
  9.8 42.1 all-gather.6
  54.1 39.2 all-gather.8
  159.7 20.3 all-gather.10
  182.1 92.3 all-gather.12
  276.5 90.4 all-gather.14
  368.9 91.2 all-gather.16
  473.7 29.3 reduce-scatter.1
where the time goes:
time: 514 us; the launch traced here: 513 us
  waiting for transfers between devices  400 us (78%)
  matrix products  62.7 us (12%)
  other arithmetic  13.9 us (3%)
  between operations  13.7 us (3%)
  blocking collectives  11.4 us (2%)
  local copies, waits for them, and re-layouts  11 us (2%)
    all_gather x1, waiting for transfers between devices, on_device(): lax.all_gather(gate_weight, 'sp', axis=0, tiled=True)  94.4 us
    all_gather x1, waiting for transfers between devices, on_device(): down_full = lax.all_gather(down_weight, 'sp', axis=1, tiled=True)  93.2 us
    all_gather x1, waiting for transfers between devices, on_device(): lax.all_gather(up_weight, 'sp', axis=0, tiled=True)  84.3 us
    all_gather x1, waiting for transfers between devices, on_device(): lax.all_gather(values, 'sp', axis=0, tiled=True)  39.8 us
    all_gather x1, waiting for transfers between devices, on_device(): lax.all_gather(key_flat, 'sp', axis=0, tiled=True)  38.1 us
    reduce_scatter x1, waiting for transfers between devices, on_device(): lax.psum_scatter(jnp.dot(hidden, down_full, preferred_element_type=jnp.fl...  29.5 us
    all_gather x1, waiting for transfers between devices, on_device(): mixer_in = lax.all_gather(normed, 'tp', axis=0, tiled=True)  18.5 us
    dot_general x4, matrix products, step(): jnp.einsum('cgqk,kcd->cgqd', exp_scores.astype(jnp.bfloat16), value_block...  18.4 us
  transfers between devices with their start and end apart: 7, of which 7 were waited for; matrix products, arithmetic and copies ran while one was open for 3% of the time, Pallas kernels for 0%

commit v1 on v0

--- a/solution.py
+++ b/solution.py
@@ -5,6 +5,10 @@
 from jax.sharding import PartitionSpec as P
 
 GRID_W = 64
+
+
+def edit_the_bands(xs, along_axis="sp"):
+    return jnp.concatenate(lax.all_gather(xs, along_axis), axis=1)
 
 
 def rms_scale(matrix):
@@ -114,7 +118,7 @@
         lax.all_gather(up_weight, "sp", axis=0, tiled=True),
         preferred_element_type=jnp.float32,
     )
-    down_full = lax.all_gather(down_weight, "sp", axis=1, tiled=True)
+    down_full = edit_the_bands(down_weight)
     hidden = (jax.nn.silu(gate_proj) * up_proj).astype(jnp.bfloat16)
     mlp_branch = lax.psum_scatter(
         jnp.dot(hidden, down_full, preferred_element_type=jnp.float32).astype(jnp.bfloat16),

time: 514 us -> 449 us (0.87)
  waiting for transfers between devices: 400 us -> 326 us
  local copies, waits for them, and re-layouts: 11 us -> 20 us
    all_gather x1, waiting for transfers between devices: 93.2 us -> 24.1 us  [edit_the_bands(): return jnp.concatenate(lax.all_gather(xs, along_axis), axis=1)]
    reshape x0 -> x1, local copies, waits for them, and re-layouts: none -> 8.32 us  [edit_the_bands(): return jnp.concatenate(lax.all_gather(xs, along_axis), axis=1)]
  transfers between devices with their start and end apart: 7 -> 7, of which waited for: 7 -> 7; matrix products, arithmetic and copies ran while one was open for 3% -> 16% of each run, Pallas kernels for 0% -> 0%
where the time goes in v1:
time: 449 us
  waiting for transfers between devices  326 us (73%)
  matrix products  63.4 us (14%)
  local copies, waits for them, and re-layouts  20 us (4%)
  other arithmetic  13.8 us (3%)
  between operations  13.7 us (3%)
  blocking collectives  11.4 us (3%)
    all_gather x1, waiting for transfers between devices, on_device(): lax.all_gather(gate_weight, 'sp', axis=0, tiled=True)  94.4 us
    all_gather x1, waiting for transfers between devices, on_device(): lax.all_gather(up_weight, 'sp', axis=0, tiled=True)  84.3 us
    all_gather x1, waiting for transfers between devices, on_device(): lax.all_gather(values, 'sp', axis=0, tiled=True)  39.8 us
    all_gather x1, waiting for transfers between devices, on_device(): lax.all_gather(key_flat, 'sp', axis=0, tiled=True)  37.3 us
    reduce_scatter x1, waiting for transfers between devices, on_device(): lax.psum_scatter(jnp.dot(hidden, down_full, preferred_element_type=jnp.fl...  29.5 us
    all_gather x1, waiting for transfers between devices, edit_the_bands(): return jnp.concatenate(lax.all_gather(xs, along_axis), axis=1)  24.1 us
    dot_general x4, matrix products, step(): jnp.einsum('cgqk,kcd->cgqd', exp_scores.astype(jnp.bfloat16), value_block...  18.8 us
    dot_general x4, matrix products, step(): jnp.einsum('qcgd,kcd->cgqk', grouped, key_block, preferred_element_type=j...  18.3 us
  transfers between devices with their start and end apart: 7, of which 7 were waited for; matrix products, arithmetic and copies ran while one was open for 16% of the time, Pallas kernels for 0%

profile of v1, /device:TPU:0, one launch (start us, length us, event | category | flops | bytes accessed | tf_op | source)
XLA Modules:
  0.0 448.8 jit_solution(11858819832367672950)
XLA Ops:
  14.6 37.3 %all-gather.8.cloned.1.call-done = bf16[4096,128]{0,1:T(8,128)(2,1)} async-done(((bf16[512,128]{0,1:T(8,128)(2,1)}), bf16[4096,128]{0,1:T(8,128)(2,1)}) %all-gather.8.cloned.1.call-update) | async-done | bytes 1048592 | tf_op jit(solution)/shard_map/all_gather | solution.py:65
  52.0 1.6 copy.32
  53.6 39.8 %all-gather.10.cloned.1.call-done = bf16[4096,128]{1,0:T(8,128)(2,1)} async-done(((bf16[512,128]{1,0:T(8,128)(2,1)}), bf16[4096,128]{1,0:T(8,128)(2,1)}) %all-gather.10.cloned.1.call-update) | async-done | bytes 1048592 | tf_op jit(solution)/shard_map/all_gather | solution.py:66
  93.4 48.8 %while.15 = (s32[]{:T(128)}, f32[1,4,512]{2,1,0:T(4,128)S(1)}, f32[1,4,512]{2,1,0:T(4,128)S(1)}, f32[1,4,512,128]{3,2,1,0:T(8,128)S(1)}, bf16[4,1024,1,128]{3,1,...) while((s32[]{:T(128)}, f32[1,4,512]{2,1,0:T(4,128)S(1)}, ...), condition=%wide.region_5.6_spmd.clone, body=%wide.region_2.5_spmd.clone.sunk | while | flops 1091317760 | bytes 61997704 | solution.py:97
  93.4 4.6 %bitcast_reduce_fusion.3 = (f32[4,512]{1,0:T(4,128)S(1)}, f32[1024,512,4]{1,0,2:T(8,128)}) fusion(bf16[512,1,4,128]{3,0,2,1:T(8,128)(2,1)S(1)} %get-tuple-element.187, bf16[4,1024,1,128]{3,1,2,0:T(8,128)(2,1)S(1)} %get-tuple-element.186, s32[]{:T(128)} %get-tuple-element.173), kind=kOutput, calls=%fused_computation.1.clone.1 | convolution fusion | flops 541063168 | bytes 9183236 | tf_op jit(solution)/shard_map/while/body/eval_jaxpr/qcgd,kcd->cgqk/dot_general | solution.py:77
  98.0 4.7 %fusion.60 = f32[1,4,512,128]{3,2,1,0:T(8,128)S(1)} fusion(f32[1024,512,4]{1,0,2:T(8,128)} %get-tuple-element.162, f32[4,512]{1,0:T(4,128)S(1)} %bitcast.106, f32[1,4,512,128]{3,2,1,0:T(8,128)S(1)} %get-tuple-element.176, f32[4,512]{1,0:T(4,128)S(1)} %get-tuple-element.163, pred[]{:T(512)S(6)} %compare.22, ...), kind=kOutput, calls=%fused_computation.10.clone.1 | convolution fusion | flops 543948800 | bytes 10764801 | tf_op jit(solution)/shard_map/while/body/eval_jaxpr/cgqk,kcd->cgqd/dot_general | solution.py:84
  102.7 1.9 copy-done
  106.1 4.6 %bitcast_reduce_fusion.3 = (f32[4,512]{1,0:T(4,128)S(1)}, f32[1024,512,4]{1,0,2:T(8,128)}) fusion(bf16[512,1,4,128]{3,0,2,1:T(8,128)(2,1)S(1)} %get-tuple-element.187, bf16[4,1024,1,128]{3,1,2,0:T(8,128)(2,1)S(1)} %get-tuple-element.186, s32[]{:T(128)} %get-tuple-element.173), kind=kOutput, calls=%fused_computation.1.clone.1 | convolution fusion | flops 541063168 | bytes 9183236 | tf_op jit(solution)/shard_map/while/body/eval_jaxpr/qcgd,kcd->cgqk/dot_general | solution.py:77
  110.6 4.6 %fusion.60 = f32[1,4,512,128]{3,2,1,0:T(8,128)S(1)} fusion(f32[1024,512,4]{1,0,2:T(8,128)} %get-tuple-element.162, f32[4,512]{1,0:T(4,128)S(1)} %bitcast.106, f32[1,4,512,128]{3,2,1,0:T(8,128)S(1)} %get-tuple-element.176, f32[4,512]{1,0:T(4,128)S(1)} %get-tuple-element.163, pred[]{:T(512)S(6)} %compare.22, ...), kind=kOutput, calls=%fused_computation.10.clone.1 | convolution fusion | flops 543948800 | bytes 10764801 | tf_op jit(solution)/shard_map/while/body/eval_jaxpr/cgqk,kcd->cgqd/dot_general | solution.py:84
  118.0 4.6 %bitcast_reduce_fusion.3 = (f32[4,512]{1,0:T(4,128)S(1)}, f32[1024,512,4]{1,0,2:T(8,128)}) fusion(bf16[512,1,4,128]{3,0,2,1:T(8,128)(2,1)S(1)} %get-tuple-element.187, bf16[4,1024,1,128]{3,1,2,0:T(8,128)(2,1)S(1)} %get-tuple-element.186, s32[]{:T(128)} %get-tuple-element.173), kind=kOutput, calls=%fused_computation.1.clone.1 | convolution fusion | flops 541063168 | bytes 9183236 | tf_op jit(solution)/shard_map/while/body/eval_jaxpr/qcgd,kcd->cgqk/dot_general | solution.py:77
  122.6 4.6 %fusion.60 = f32[1,4,512,128]{3,2,1,0:T(8,128)S(1)} fusion(f32[1024,512,4]{1,0,2:T(8,128)} %get-tuple-element.162, f32[4,512]{1,0:T(4,128)S(1)} %bitcast.106, f32[1,4,512,128]{3,2,1,0:T(8,128)S(1)} %get-tuple-element.176, f32[4,512]{1,0:T(4,128)S(1)} %get-tuple-element.163, pred[]{:T(512)S(6)} %compare.22, ...), kind=kOutput, calls=%fused_computation.10.clone.1 | convolution fusion | flops 543948800 | bytes 10764801 | tf_op jit(solution)/shard_map/while/body/eval_jaxpr/cgqk,kcd->cgqd/dot_general | solution.py:84
  130.0 4.6 %bitcast_reduce_fusion.3 = (f32[4,512]{1,0:T(4,128)S(1)}, f32[1024,512,4]{1,0,2:T(8,128)}) fusion(bf16[512,1,4,128]{3,0,2,1:T(8,128)(2,1)S(1)} %get-tuple-element.187, bf16[4,1024,1,128]{3,1,2,0:T(8,128)(2,1)S(1)} %get-tuple-element.186, s32[]{:T(128)} %get-tuple-element.173), kind=kOutput, calls=%fused_computation.1.clone.1 | convolution fusion | flops 541063168 | bytes 9183236 | tf_op jit(solution)/shard_map/while/body/eval_jaxpr/qcgd,kcd->cgqk/dot_general | solution.py:77
  134.6 4.8 %fusion.60 = f32[1,4,512,128]{3,2,1,0:T(8,128)S(1)} fusion(f32[1024,512,4]{1,0,2:T(8,128)} %get-tuple-element.162, f32[4,512]{1,0:T(4,128)S(1)} %bitcast.106, f32[1,4,512,128]{3,2,1,0:T(8,128)S(1)} %get-tuple-element.176, f32[4,512]{1,0:T(4,128)S(1)} %get-tuple-element.163, pred[]{:T(512)S(6)} %compare.22, ...), kind=kOutput, calls=%fused_computation.10.clone.1 | convolution fusion | flops 543948800 | bytes 10764801 | tf_op jit(solution)/shard_map/while/body/eval_jaxpr/cgqk,kcd->cgqd/dot_general | solution.py:84
  143.1 11.4 %all_to_all.16 = bf16[4,128,512]{2,1,0:T(8,128)(2,1)S(1)} all-to-all(bf16[4,128,512]{2,1,0:T(8,128)(2,1)S(1)} %convert_element_type.88), channel_id=1, replica_groups=mesh['sp'=8,'tp'=4] {'tp'}, dimensions={0} | all-to-all | bytes 1048576 | tf_op jit(solution)/shard_map/all_to_all | solution.py:104
  154.9 4.8 %multiply_reduce_fusion = (f32[128]{0:T(128)S(1)}, f32[128,2048]{1,0:T(8,128)S(1)}) fusion(bf16[128,2048]{0,1:T(8,128)(2,1)S(1)} %bitcast.109, bf16[2048,2048]{1,0:T(8,128)(2,1)} %param.20), kind=kOutput, calls=%fused_computation.42 | convolution fusion | flops 1074265984 | bytes 9961984 | tf_op jit(solution)/shard_map/dot_general | solution.py:105
  162.5 24.1 %all-gather.18.cloned.1.call-done = bf16[11264,256]{1,0:T(8,128)(2,1)} async-done(((bf16[1408,256]{1,0:T(8,128)(2,1)}), bf16[11264,256]{1,0:T(8,128)(2,1)}) %all-gather.18.cloned.1.call-update) | async-done | bytes 5767184 | tf_op jit(solution)/shard_map/all_gather | solution.py:11
  186.7 8.3 %copy.30 = bf16[1408,8,256]{0,2,1:T(8,128)(2,1)} copy(bf16[1408,8,256]{2,0,1:T(8,128)(2,1)} %bitcast.103) | data formatting | bytes 11534336 | tf_op jit(solution)/shard_map/reshape | solution.py:11
  195.0 13.9 %all-gather.12.cloned.1.call-done = bf16[512,2048]{1,0:T(8,128)(2,1)} async-done(((bf16[128,2048]{1,0:T(8,128)(2,1)}), bf16[512,2048]{1,0:T(8,128)(2,1)}) %all-gather.12.cloned.1.call-update) | async-done | bytes 2097168 | tf_op jit(solution)/shard_map/all_gather | solution.py:110
  208.8 94.4 %all-gather.14.cloned.1.call-done = bf16[2048,1408]{1,0:T(8,128)(2,1)} async-done(((bf16[256,1408]{1,0:T(8,128)(2,1)}), bf16[2048,1408]{1,0:T(8,128)(2,1)}) %all-gather.14.cloned.1.call-update) | async-done | bytes 5767184 | tf_op jit(solution)/shard_map/all_gather | solution.py:113
  303.2 8.3 %fusion.43 = f32[512,1408]{1,0:T(8,128)} fusion(bf16[512,2048]{1,0:T(8,128)(2,1)} %all-gather.12.cloned.1.call-done, bf16[2048,1408]{1,0:T(8,128)(2,1)} %all-gather.14.cloned.1.call-done), kind=kOutput, calls=%fused_computation.81 | convolution fusion | flops 2952790016 | bytes 10747904 | tf_op jit(solution)/shard_map/dot_general | solution.py:111
  311.5 84.3 %all-gather.16.cloned.1.call-done = bf16[2048,1408]{1,0:T(8,128)(2,1)} async-done(((bf16[256,1408]{1,0:T(8,128)(2,1)}), bf16[2048,1408]{1,0:T(8,128)(2,1)}) %all-gather.16.cloned.1.call-update) | async-done | bytes 5767184 | tf_op jit(solution)/shard_map/all_gather | solution.py:118
  395.8 13.3 %convolution_convert_fusion = bf16[512,2048]{1,0:T(8,128)(2,1)} fusion(bf16[1408,2048]{0,1:T(8,128)(2,1)} %bitcast.104, bf16[512,2048]{1,0:T(8,128)(2,1)S(1)} %copy-done.5, bf16[2048,1408]{1,0:T(8,128)(2,1)} %all-gather.16.cloned.1.call-done, f32[512,1408]{1,0:T(8,128)} %fusion.43), kind=kOutput, calls=%fused_computation.28 | convolution fusion | flops 5910953984 | bytes 18612224 | tf_op jit(solution)/shard_map/dot_general | solution.py:124
  409.1 29.5 %reduce-scatter.2.cloned.1.call-done = bf16[128,2048]{1,0:T(8,128)(2,1)} async-done(((bf16[512,2048]{1,0:T(8,128)(2,1)}), bf16[128,2048]{1,0:T(8,128)(2,1)}) %reduce-scatter.2.cloned.1.call-update) | async-done | bytes 524304 | tf_op jit(solution)/shard_map/reduce_scatter | solution.py:123
  439.8 2.1 fusion.30
  (78 shorter events, 22.8 us)
Async XLA Ops:
  6.5 45.4 %all-gather.8.cloned.1.call-start = ((), (), s32[]{:S(2)}) async-start(), calls=%async_computation.2 | async-start | bytes 1179648 | tf_op jit(solution)/shard_map/all_gather | solution.py:65
  9.7 83.7 %all-gather.10.cloned.1.call-start = ((), (), s32[]{:S(2)}) async-start(), calls=%async_computation.3 | async-start | bytes 1179648 | tf_op jit(solution)/shard_map/all_gather | solution.py:66
  10.4 176.2 %all-gather.18.cloned.1.call-start = ((), (), s32[]{:S(2)}) async-start(), calls=%async_computation.8 | async-start | bytes 6488064 | tf_op jit(solution)/shard_map/all_gather | solution.py:11
  11.2 197.7 %all-gather.12.cloned.1.call-start = ((), (), s32[]{:S(2)}) async-start(), calls=%async_computation.4 | async-start | bytes 2621440 | tf_op jit(solution)/shard_map/all_gather | solution.py:110
  98.0 6.7 %copy-start = (f32[1024,512,4]{1,0,2:T(8,128)S(1)}, f32[1024,512,4]{1,0,2:T(8,128)}, u32[]{:S(2)}) copy-start(f32[1024,512,4]{1,0,2:T(8,128)} %get-tuple-element.162) | copy-start | bytes 25165828 | tf_op jit(solution)/shard_map/while
  110.6 6.0 %copy-start = (f32[1024,512,4]{1,0,2:T(8,128)S(1)}, f32[1024,512,4]{1,0,2:T(8,128)}, u32[]{:S(2)}) copy-start(f32[1024,512,4]{1,0,2:T(8,128)} %get-tuple-element.162) | copy-start | bytes 25165828 | tf_op jit(solution)/shard_map/while
  122.6 5.9 %copy-start = (f32[1024,512,4]{1,0,2:T(8,128)S(1)}, f32[1024,512,4]{1,0,2:T(8,128)}, u32[]{:S(2)}) copy-start(f32[1024,512,4]{1,0,2:T(8,128)} %get-tuple-element.162) | copy-start | bytes 25165828 | tf_op jit(solution)/shard_map/while
  134.5 6.2 %copy-start = (f32[1024,512,4]{1,0,2:T(8,128)S(1)}, f32[1024,512,4]{1,0,2:T(8,128)}, u32[]{:S(2)}) copy-start(f32[1024,512,4]{1,0,2:T(8,128)} %get-tuple-element.162) | copy-start | bytes 25165828 | tf_op jit(solution)/shard_map/while
  154.9 4.8 %copy-start.1 = (bf16[128,2048]{1,0:T(8,128)(2,1)S(1)}, bf16[128,2048]{1,0:T(8,128)(2,1)}, u32[]{:S(2)}) copy-start(bf16[128,2048]{1,0:T(8,128)(2,1)} %param.22) | copy-start | bytes 1572868
  154.9 4.8 %copy-start.2 = (f32[2048]{0:T(1024)S(1)}, f32[2048]{0:T(1024)}, u32[]{:S(2)}) copy-start(f32[2048]{0:T(1024)} %param.21) | copy-start | bytes 24580
  154.9 5.2 %copy-start.3 = (f32[2048]{0:T(1024)S(1)}, f32[2048]{0:T(1024)}, u32[]{:S(2)}) copy-start(f32[2048]{0:T(1024)} %param.23) | copy-start | bytes 24580
  161.1 142.1 %all-gather.14.cloned.1.call-start = ((), (), s32[]{:S(2)}) async-start(), calls=%async_computation.5 | async-start | bytes 6488064 | tf_op jit(solution)/shard_map/all_gather | solution.py:113
  161.7 234.1 %all-gather.16.cloned.1.call-start = ((), (), s32[]{:S(2)}) async-start(), calls=%async_computation.6 | async-start | bytes 6488064 | tf_op jit(solution)/shard_map/all_gather | solution.py:118
  162.3 276.3 %reduce-scatter.2.cloned.1.call-start = ((), (), s32[]{:S(2)}) async-start(), calls=%async_computation.7 | async-start | bytes 2621440 | tf_op jit(solution)/shard_map/reduce_scatter | solution.py:123
  208.8 186.9 %copy-start.5 = (bf16[512,2048]{1,0:T(8,128)(2,1)S(1)}, bf16[512,2048]{1,0:T(8,128)(2,1)}, u32[]{:S(2)}) copy-start(bf16[512,2048]{1,0:T(8,128)(2,1)} %all-gather.12.cloned.1.call-done) | copy-start | bytes 6291460
  395.8 44.1 %copy-start.4 = (f32[2048]{0:T(1024)S(1)}, f32[2048]{0:T(1024)}, u32[]{:S(2)}) copy-start(f32[2048]{0:T(1024)} %param.27) | copy-start | bytes 24580
Sparse Core Ops, SparseCore 0:
  9.8 42.1 all-gather.7
  54.1 39.2 all-gather.9
  95.6 91.0 all-gather.17
  188.1 20.7 all-gather.11
  210.9 92.3 all-gather.13
  305.3 90.4 all-gather.15
  409.2 29.3 reduce-scatter.1
